TPU v7x, 32 devices: a whole 2x2x4 slice. The times are simulated.
32 devices in a mesh: ep: 8 (over z, x), tp: 4 (over y, core).
Axes of the slice: x: 2, y: 2, z: 4, core: 2. Of those that a mesh axis runs over, the one named last changes fastest.
Arguments:
- tokens: bfloat16 [1024, 2048], P('ep'), may hold values from -6 to 6
- chosen: int32 [8, 8, 7], P('ep'), may hold values from -1 to 127, as said below
- pick_weight: float32 [8, 8, 7], P('ep'), may hold values from 0.2 to 1
- gate_weight: bfloat16 [8, 2048, 4096], P('ep', None, 'tp'), may hold values from -0.125 to 0.125
- up_weight: bfloat16 [8, 2048, 4096], P('ep', None, 'tp'), may hold values from -0.125 to 0.125
- down_weight: bfloat16 [8, 4096, 2048], P('ep', 'tp'), may hold values from -0.09375 to 0.09375
Outputs:
- combined: bfloat16 [1024, 2048], P('ep', 'tp')
Inputs may be any that keep to these rules, and one draw needn't show every extreme that they name: `chosen`: within one group and one expert the named positions are distinct, and the filled slots come first. From each group every expert takes at least 3 tokens and at most 7; every expert takes exactly 7 tokens from some group, and exactly 40 tokens in all.
All inputs are finite; a program needn't handle non-finite values.
Results may differ from a plain program's by a relative error of at most 0.019.
Values may be sent and summed in bfloat16 or wider, within the bound.
A program may use at most 64 MiB of HBM per device.

v0:
```python
import jax
import jax.numpy as jnp
from jax import lax
from jax.sharding import PartitionSpec as P


def on_device(tokens, chosen, pick_weight, gate_weight, up_weight, down_weight):
    model_width = tokens.shape[1]
    experts = chosen.shape[1]
    slot_count = chosen.shape[2]
    chosen_ids = chosen[0]
    filled = chosen_ids >= 0
    safe_ids = jnp.where(filled, chosen_ids, 0).reshape(-1)
    picked = jnp.take(tokens, safe_ids, axis=0)
    picked = jnp.where(filled.reshape(-1, 1), picked, jnp.zeros((), tokens.dtype))
    picked = picked.reshape(experts, slot_count, model_width)
    received = lax.all_to_all(picked, "ep", split_axis=0, concat_axis=0, tiled=True)
    expert_rows = received.reshape(-1, model_width)
    gate_pre = jnp.dot(expert_rows, gate_weight[0], preferred_element_type=jnp.float32)
    up_pre = jnp.dot(expert_rows, up_weight[0], preferred_element_type=jnp.float32)
    hidden = (jax.nn.silu(gate_pre) * up_pre).astype(jnp.bfloat16)
    down_local = down_weight[0]
    summed = lax.psum_scatter(
        jnp.einsum("fd,rf->dr", down_local, hidden, preferred_element_type=jnp.float32).astype(
            jnp.bfloat16
        ),
        "tp",
        scatter_dimension=0,
        tiled=True,
    )
    returned = lax.all_to_all(summed, "ep", split_axis=1, concat_axis=1, tiled=True)
    weights = jnp.where(filled, pick_weight[0], jnp.zeros((), jnp.float32)).reshape(-1)
    positions = lax.iota(jnp.int32, tokens.shape[0])
    onehot = jnp.where(
        positions[:, None] == safe_ids[None, :], weights[None, :], jnp.zeros((), jnp.float32)
    )
    combined = jnp.einsum(
        "tk,wk->tw",
        onehot,
        returned.astype(jnp.float32),
        precision=lax.Precision.HIGHEST,
        preferred_element_type=jnp.float32,
    )
    return combined.astype(jnp.bfloat16)


def solution(mesh):
    return jax.shard_map(
        on_device,
        mesh=mesh,
        in_specs=(
            P("ep", None),
            P("ep", None, None),
            P("ep", None, None),
            P("ep", None, "tp"),
            P("ep", None, "tp"),
            P("ep", "tp", None),
        ),
        out_specs=P("ep", "tp"),
        check_vma=False,
    )
```

profile of v0, /device:TPU:0, one launch (start us, length us, event | category | flops | bytes accessed | tf_op | source)
XLA Modules:
  0.0 74.2 jit_solution(4793843722620870495)
XLA Ops:
  6.5 0.0 copy-start
  6.5 0.0 reduce-scatter.2.cloned.1.call-start
  6.5 0.8 %copy.11 = s32[1,8,7]{2,1,0:T(8,128)S(1)} copy(s32[1,8,7]{1,0,2:T(1,128)} %param.7) | data formatting | bytes 448 | tf_op args[1]
  7.4 0.1 squeeze.22
  7.5 0.1 copy-done
  7.6 0.7 gather_fusion
  8.3 0.1 gather.7
  8.4 0.1 select_select_fusion
  8.5 16.0 %all_to_all.17 = bf16[8,7,2048]{2,1,0:T(8,128)(2,1)S(1)} all-to-all(bf16[8,7,2048]{2,1,0:T(8,128)(2,1)S(1)} %select_select_fusion), channel_id=1, replica_groups=mesh['ep'=8,'tp'=4] {'ep'}, dimensions={0} | all-to-all | bytes 458752 | tf_op jit(solution)/shard_map/all_to_all | solution.py:17
  24.5 0.1 reshape.74
  24.6 3.0 %fusion.4 = f32[56,1024]{1,0:T(8,128)S(1)} fusion(bf16[56,2048]{1,0:T(8,128)(2,1)S(1)} %reshape.74, bf16[1,2048,1024]{2,1,0:T(8,128)(2,1)} %param.9), kind=kOutput, calls=%fused_computation.5 | convolution fusion | flops 234881024 | bytes 4653056 | tf_op jit(solution)/shard_map/dot_general | solution.py:19
  27.6 0.0 copy-start.1
  27.6 5.7 %fusion.9 = bf16[2048,56]{0,1:T(8,128)(2,1)} fusion(bf16[1,1024,2048]{2,1,0:T(8,128)(2,1)} %param.11, bf16[56,2048]{1,0:T(8,128)(2,1)S(1)} %reshape.74, bf16[1,2048,1024]{2,1,0:T(8,128)(2,1)} %param.10, f32[56,1024]{1,0:T(8,128)S(1)} %fusion.4), kind=kOutput, calls=%fused_computation.8 | convolution fusion | flops 470220800 | bytes 9076736 | tf_op jit(solution)/shard_map/fd,rf->dr/dot_general | solution.py:24
  33.4 0.0 reduce-scatter.2.cloned.1.call-update
  33.4 0.1 squeeze.19
  33.5 0.0 copy-done.1
  33.5 0.1 copy.12
  33.5 0.1 squeeze.20
  33.6 18.9 %reduce-scatter.2.cloned.1.call-done = bf16[512,56]{0,1:T(8,128)(2,1)} async-done(((bf16[2048,56]{0,1:T(8,128)(2,1)}), bf16[512,56]{0,1:T(8,128)(2,1)}) %reduce-scatter.2.cloned.1.call-update) | async-done | bytes 57360 | tf_op jit(solution)/shard_map/reduce_scatter | solution.py:23
  52.5 1.5 %all_to_all.12 = bf16[512,8,7]{0,2,1:T(8,128)(2,1)} reshape(bf16[512,56]{0,1:T(8,128)(2,1)} %reduce-scatter.2.cloned.1.call-done) | data formatting | bytes 114688 | tf_op jit(solution)/shard_map/all_to_all | solution.py:31
  54.0 5.5 %all-to-all-start.1 = ((bf16[512,8,7]{0,2,1:T(8,128)(2,1)}), bf16[512,8,7]{0,2,1:T(8,128)(2,1)S(1)}, u32[]{:S(2)}, u32[]{:S(2)}) async-start(bf16[512,8,7]{0,2,1:T(8,128)(2,1)} %all_to_all.12), calls=%async_computation.2 | async-start | bytes 131072 | tf_op jit(solution)/shard_map/all_to_all | solution.py:31
  59.5 6.9 %all-to-all-done.1 = bf16[512,8,7]{0,2,1:T(8,128)(2,1)S(1)} async-done(((bf16[512,8,7]{0,2,1:T(8,128)(2,1)}), bf16[512,8,7]{0,2,1:T(8,128)(2,1)S(1)}, u32[]{:S(2)}, u32[]{:S(2)}) %all-to-all-start.1) | async-done | bytes 57376 | tf_op jit(solution)/shard_map/all_to_all | solution.py:31
  66.4 0.9 %convolution_convert_fusion = bf16[128,512]{1,0:T(8,128)(2,1)} fusion(bf16[512,56]{0,1:T(8,128)(2,1)S(1)} %all_to_all.14, f32[56]{0:T(128)S(1)} %compare_select_fusion.3, s32[56]{0:T(128)S(1)} %compare_select_fusion.4), kind=kOutput, calls=%fused_computation.10 | convolution fusion | flops 44120064 | bytes 188864 | tf_op jit(solution)/shard_map/tk,wk->tw/dot_general | solution.py:37
  (6 shorter events, 0.1 us)
Async XLA Ops:
  6.5 1.1 %copy-start = (bf16[128,2048]{1,0:T(8,128)(2,1)S(1)}, bf16[128,2048]{1,0:T(8,128)(2,1)}, u32[]{:S(2)}) copy-start(bf16[128,2048]{1,0:T(8,128)(2,1)} %param.6) | copy-start | bytes 1572868
  6.5 46.0 %reduce-scatter.2.cloned.1.call-start = ((), (), s32[]{:S(2)}) async-start(), calls=%async_computation.3 | async-start | bytes 286720 | tf_op jit(solution)/shard_map/reduce_scatter | solution.py:23
  27.6 5.8 %copy-start.1 = (f32[1,8,7]{1,0,2:T(1,128)S(1)}, f32[1,8,7]{1,0,2:T(1,128)}, u32[]{:S(2)}) copy-start(f32[1,8,7]{1,0,2:T(1,128)} %param.8) | copy-start | bytes 676
  54.0 12.4 %all-to-all-start.1 = ((bf16[512,8,7]{0,2,1:T(8,128)(2,1)}), bf16[512,8,7]{0,2,1:T(8,128)(2,1)S(1)}, u32[]{:S(2)}, u32[]{:S(2)}) async-start(bf16[512,8,7]{0,2,1:T(8,128)(2,1)} %all_to_all.12), calls=%async_computation.2 | async-start | bytes 131072 | tf_op jit(solution)/shard_map/all_to_all | solution.py:31
Sparse Core Ops, SparseCore 0:
  33.5 18.9 reduce-scatter.1
where the time goes:
time: 74.5 us; the launch traced here: 74.2 us
  waiting for transfers between devices  25.8 us (35%)
  blocking collectives  16 us (21%)
  between operations  13.4 us (18%)
  matrix products  9.65 us (13%)
  starting transfers between devices  5.5 us (7%)
  local copies, waits for them, and re-layouts  3.66 us (5%)
    reduce_scatter x1, waiting for transfers between devices, on_device(): lax.psum_scatter(jnp.einsum('fd,rf->dr', down_local, hidden, preferred_el...  18.9 us
    all_to_all x1, blocking collectives, on_device(): lax.all_to_all(picked, 'ep', split_axis=0, concat_axis=0, tiled=True)  16 us
    all_to_all x1, waiting for transfers between devices, on_device(): lax.all_to_all(summed, 'ep', split_axis=1, concat_axis=1, tiled=True)  6.9 us
    dot_general x1, matrix products, on_device(): jnp.einsum('fd,rf->dr', down_local, hidden, preferred_element_type=jnp.fl...  5.72 us
    all_to_all x1, starting transfers between devices, on_device(): lax.all_to_all(summed, 'ep', split_axis=1, concat_axis=1, tiled=True)  5.5 us
    dot_general x1, matrix products, on_device(): jnp.dot(expert_rows, gate_weight[0], preferred_element_type=jnp.float32)  3.02 us
    all_to_all x2, local copies, waits for them, and re-layouts, on_device(): lax.all_to_all(summed, 'ep', split_axis=1, concat_axis=1, tiled=True)  1.51 us
  transfers between devices with their start and end apart: 2, of which 2 were waited for; matrix products, arithmetic and copies ran while one was open for 0% of the time, Pallas kernels for 0%

commit v1 on v0

v1 whole, which is shorter than its diff:
```python
import functools
import jax
import jax.numpy as jnp
from jax import lax
from jax.experimental import pallas as pl
from jax.experimental.pallas import tpu as pltpu
from jax.sharding import PartitionSpec as P

F32 = jnp.float32
BF16 = jnp.bfloat16
PAD = 8


def each(n, f):
    if n <= 16:
        for i in range(n):
            f(i)
    else:
        lax.fori_loop(0, n, lambda i, s: (f(i), s)[1], 0)


def layer(
    ep, tp, tok_hbm, cho_hbm, pw_hbm, gate_hbm, up_hbm, down_hbm, out_ref,
    tok, cho, pw, gate, up, down, send1, x_own, x_sib, acc_g, acc_u, hid,
    send2, recv2, mine, send3, recv3, comb,
    in_sem, w_sem, s1_sem, r1_sem, s2_sem, r2_sem, s3_sem, r3_sem, s4_sem, r4_sem,
):
    slots = cho.shape[2]
    toks, half = tok.shape
    hidden = hid.shape[1]
    blk = out_ref.shape[1]
    ny = tp // 2
    e_me = lax.axis_index("ep")
    t_me = lax.axis_index("tp")
    y_me, c_me = t_me // 2, t_me % 2
    sib = y_me * 2 + (1 - c_me)
    own_k = pl.multiple_of(c_me * half, 128)
    sib_k = pl.multiple_of((1 - c_me) * half, 128)

    small = [
        pltpu.make_async_copy(cho_hbm, cho, in_sem.at[0]),
        pltpu.make_async_copy(pw_hbm, pw, in_sem.at[1]),
        pltpu.make_async_copy(tok_hbm.at[:, pl.ds(own_k, half)], tok, in_sem.at[2]),
    ]
    for c in small:
        c.start()

    barrier = pltpu.get_barrier_semaphore()
    group = ep * ny
    me = e_me * ny + y_me

    def greet(k):
        at = lax.rem(me + k + 1, group)
        pl.semaphore_signal(
            barrier, inc=1, device_id={"ep": at // ny, "tp": lax.rem(at, ny) * 2 + c_me},
            device_id_type=pl.DeviceIdType.MESH)

    each(group - 1, greet)
    pl.semaphore_signal(
        barrier, inc=1, device_id={"tp": sib}, device_id_type=pl.DeviceIdType.MESH)

    weights = [
        pltpu.make_async_copy(gate_hbm.at[0, pl.ds(own_k, half)], gate.at[pl.ds(own_k, half)], w_sem.at[0]),
        pltpu.make_async_copy(up_hbm.at[0, pl.ds(own_k, half)], up.at[pl.ds(own_k, half)], w_sem.at[1]),
        pltpu.make_async_copy(gate_hbm.at[0, pl.ds(sib_k, half)], gate.at[pl.ds(sib_k, half)], w_sem.at[2]),
        pltpu.make_async_copy(up_hbm.at[0, pl.ds(sib_k, half)], up.at[pl.ds(sib_k, half)], w_sem.at[3]),
        pltpu.make_async_copy(down_hbm.at[0], down, w_sem.at[4]),
    ]
    for c in weights:
        c.start()

    small[0].wait()
    small[1].wait()
    shape = (PAD, slots)
    diag = lax.broadcasted_iota(jnp.int32, shape, 0) == lax.broadcasted_iota(jnp.int32, shape, 1)
    here = lax.broadcasted_iota(jnp.int32, (PAD, toks), 1)
    last = lax.broadcasted_iota(jnp.int32, (PAD, 1), 0) >= slots
    hot, wgt = [], []
    for e in range(ep):
        ids = jnp.broadcast_to(cho[0, e:e + 1, :], shape)
        val = jnp.broadcast_to(pw[0, e:e + 1, :], shape)
        ids = jnp.sum(jnp.where(diag, ids, 0), axis=1, keepdims=True)
        val = jnp.sum(jnp.where(diag, val, 0.0), axis=1, keepdims=True)
        ids = jnp.where(last, -1, ids)
        hit = here == ids
        hot.append(jnp.where(hit, 1.0, 0.0))
        wgt.append(jnp.where(hit, val, 0.0))
    hot = jnp.concatenate(hot, axis=0).astype(BF16)
    small[2].wait()
    picked = jnp.dot(hot, tok[...], preferred_element_type=F32)
    send1[...] = picked.reshape(ep, PAD, half).astype(BF16)
    x_own[e_me] = send1[e_me]

    pl.semaphore_wait(barrier, group)

    def copy1(k):
        to = lax.rem(e_me + k, ep)
        return pltpu.make_async_remote_copy(
            src_ref=send1.at[to], dst_ref=x_own.at[e_me], send_sem=s1_sem, recv_sem=r1_sem.at[e_me],
            device_id={"ep": to}, device_id_type=pl.DeviceIdType.MESH)

    each(ep - 1, lambda i: copy1(lax.rem(i + ep // 2 - 1, ep - 1) + 1).start())

    wgt = jnp.concatenate(wgt, axis=0)
    hi = wgt.astype(BF16).astype(F32)
    mid = (wgt - hi).astype(BF16).astype(F32)
    lo = (wgt - hi) - mid
    comb[...] = jnp.transpose(jnp.concatenate([hi, mid, lo], axis=0)).astype(BF16)

    def relay(k):
        src = lax.rem(e_me + k, ep)
        @pl.when(k > 0)
        def _():
            pltpu.make_async_remote_copy(
                src_ref=send1.at[src], dst_ref=x_own.at[src], send_sem=s1_sem, recv_sem=r1_sem.at[src],
                device_id={"ep": src}, device_id_type=pl.DeviceIdType.MESH).wait_recv()
        pltpu.make_async_remote_copy(
            src_ref=x_own.at[src], dst_ref=x_sib.at[src], send_sem=s2_sem, recv_sem=r2_sem,
            device_id={"tp": sib}, device_id_type=pl.DeviceIdType.MESH).start()

    each(ep, relay)

    def rows(ref):
        return ref[...].astype(F32).reshape(ep * PAD, ref.shape[-1]).astype(BF16)

    step = min(256, hidden)
    x = rows(x_own)
    weights[0].wait()
    weights[1].wait()
    for j in range(0, hidden, step):
        acc_g[:, j:j + step] = jnp.dot(x, gate[pl.ds(own_k, half), j:j + step], preferred_element_type=F32)
        acc_u[:, j:j + step] = jnp.dot(x, up[pl.ds(own_k, half), j:j + step], preferred_element_type=F32)
    pltpu.make_async_remote_copy(
        src_ref=x_own, dst_ref=x_sib, send_sem=s2_sem, recv_sem=r2_sem,
        device_id={"tp": sib}, device_id_type=pl.DeviceIdType.MESH).wait_recv()
    x = rows(x_sib)
    weights[2].wait()
    weights[3].wait()
    for j in range(0, hidden, step):
        g = acc_g[:, j:j + step] + jnp.dot(x, gate[pl.ds(sib_k, half), j:j + step], preferred_element_type=F32)
        u = acc_u[:, j:j + step] + jnp.dot(x, up[pl.ds(sib_k, half), j:j + step], preferred_element_type=F32)
        hid[:, j:j + step] = (g / (1.0 + jnp.exp(-g)) * u).astype(BF16)
    h = hid[...]
    weights[4].wait()

    def part(f):
        return jnp.dot(h, down[:, pl.ds(pl.multiple_of(f * blk, 128), blk)], preferred_element_type=F32)

    def pair_copy(i):
        return pltpu.make_async_remote_copy(
            src_ref=send2.at[i], dst_ref=recv2.at[i], send_sem=s3_sem.at[i], recv_sem=r3_sem.at[i],
            device_id={"tp": sib}, device_id_type=pl.DeviceIdType.MESH)

    for i in range(ny):
        y = lax.rem(y_me + 1 + i, ny)
        send2[i] = part(y * 2 + (1 - c_me)).astype(BF16)
        pair_copy(i).start()
    for i in range(ny):
        y = lax.rem(y_me + 1 + i, ny)
        mine[...] = part(y * 2 + c_me)
        pair_copy(i).wait_recv()
        total = mine[...] + recv2[i].astype(F32)
        send3[i] = total.reshape(ep, PAD, blk).astype(BF16)

        def give(k, i=i, y=y):
            to = lax.rem(e_me + k, ep)
            pltpu.make_async_remote_copy(
                src_ref=send3.at[i, to], dst_ref=recv3.at[y_me, e_me], send_sem=s4_sem, recv_sem=r4_sem,
                device_id={"ep": to, "tp": y * 2 + c_me}, device_id_type=pl.DeviceIdType.MESH).start()

        if i == ny - 1:
            each(ep - 1, lambda k: give(lax.rem(k + ep // 2 - 1, ep - 1) + 1))
            pltpu.make_async_copy(send3.at[i, e_me], recv3.at[y_me, e_me], r4_sem).start()
        else:
            each(ep, lambda k: give(lax.rem(k + ep // 2, ep)))

    pltpu.make_async_copy(send1.at[pl.ds(0, ep - 1)], send1.at[pl.ds(0, ep - 1)], s1_sem).wait()
    pltpu.make_async_copy(x_own, x_own, s2_sem).wait()
    for i in range(ny):
        pair_copy(i).wait_send()
    pltpu.make_async_copy(recv3, recv3, r4_sem).wait()
    total = recv3[0].astype(F32)
    for y in range(1, ny):
        total = total + recv3[y].astype(F32)
    r = total.reshape(ep * PAD, blk).astype(BF16)
    out_ref[...] = jnp.dot(
        comb[...], jnp.concatenate([r, r, r], axis=0), preferred_element_type=F32).astype(BF16)
    if ny > 1:
        pltpu.make_async_copy(send3.at[pl.ds(0, ny - 1)], send3.at[pl.ds(0, ny - 1)], s4_sem).wait()
    pltpu.make_async_copy(send3.at[0, pl.ds(0, ep - 1)], send3.at[0, pl.ds(0, ep - 1)], s4_sem).wait()


def on_device(ep, tp, tokens, chosen, pick_weight, gate_weight, up_weight, down_weight):
    toks, width = tokens.shape
    hidden = gate_weight.shape[2]
    half, blk, ny, rows = width // 2, width // tp, tp // 2, ep * PAD
    dma = pltpu.SemaphoreType.DMA
    return pl.pallas_call(
        functools.partial(layer, ep, tp),
        out_shape=jax.ShapeDtypeStruct((toks, blk), tokens.dtype),
        in_specs=[pl.BlockSpec(memory_space=pl.ANY)] * 6,
        out_specs=pl.BlockSpec(memory_space=pltpu.VMEM),
        scratch_shapes=[
            pltpu.VMEM((toks, half), BF16),
            pltpu.VMEM(chosen.shape, jnp.int32),
            pltpu.VMEM(pick_weight.shape, F32),
            pltpu.VMEM((width, hidden), BF16),
            pltpu.VMEM((width, hidden), BF16),
            pltpu.VMEM((hidden, width), BF16),
            pltpu.VMEM((ep, PAD, half), BF16),
            pltpu.VMEM((ep, PAD, half), BF16),
            pltpu.VMEM((ep, PAD, half), BF16),
            pltpu.VMEM((rows, hidden), F32),
            pltpu.VMEM((rows, hidden), F32),
            pltpu.VMEM((rows, hidden), BF16),
            pltpu.VMEM((ny, rows, blk), BF16),
            pltpu.VMEM((ny, rows, blk), BF16),
            pltpu.VMEM((rows, blk), F32),
            pltpu.VMEM((ny, ep, PAD, blk), BF16),
            pltpu.VMEM((ny, ep, PAD, blk), BF16),
            pltpu.VMEM((toks, 3 * rows), BF16),
            dma((3,)), dma((5,)), dma, dma((ep,)), dma, dma, dma((ny,)), dma((ny,)), dma, dma,
        ],
        compiler_params=pltpu.CompilerParams(
            collective_id=0, has_side_effects=True, vmem_limit_bytes=60 * 1024 * 1024),
    )(tokens, chosen, pick_weight, gate_weight, up_weight, down_weight)


def solution(mesh):
    ep, tp = mesh.shape["ep"], mesh.shape["tp"]
    return jax.shard_map(
        functools.partial(on_device, ep, tp),
        mesh=mesh,
        in_specs=(
            P("ep", None),
            P("ep", None, None),
            P("ep", None, None),
            P("ep", None, "tp"),
            P("ep", None, "tp"),
            P("ep", "tp", None),
        ),
        out_specs=P("ep", "tp"),
        check_vma=False,
    )
```

time: 74.5 us -> 25.7 us (0.34)
  waiting for transfers between devices: 25.8 us -> 0 us
  Pallas kernels: 0 us -> 21.2 us
  blocking collectives: 16 us -> 0 us
  between operations: 13.4 us -> 0.01 us
  matrix products: 9.65 us -> 0 us
  starting transfers between devices: 5.5 us -> 0 us
    pallas_call x0 -> x1, Pallas kernels: none -> 21.2 us  [on_device(): pl.pallas_call(functools.partial(layer, ep, tp), out_shape=jax.ShapeDtype...]
    reduce_scatter x1 -> x0, waiting for transfers between devices: 18.9 us -> none  [on_device(): lax.psum_scatter(jnp.einsum('fd,rf->dr', down_local, hidden, preferred_el...]
    all_to_all x1 -> x0, blocking collectives: 16 us -> none  [on_device(): lax.all_to_all(picked, 'ep', split_axis=0, concat_axis=0, tiled=True)]
    dot_general x3 -> x0, matrix products: 9.65 us -> none  [the longest x1 5.72 us: on_device(): jnp.einsum('fd,rf->dr', down_local, hidden, preferred_element_type=jnp.fl...]
    all_to_all x1 -> x0, waiting for transfers between devices: 6.9 us -> none  [on_device(): lax.all_to_all(summed, 'ep', split_axis=1, concat_axis=1, tiled=True)]
    all_to_all x1 -> x0, starting transfers between devices: 5.5 us -> none  [on_device(): lax.all_to_all(summed, 'ep', split_axis=1, concat_axis=1, tiled=True)]
    unnamed x6 -> x3, local copies, waits for them, and re-layouts: 1.03 us -> 4.26 us
    all_to_all x2 -> x0, local copies, waits for them, and re-layouts: 1.51 us -> none  [on_device(): lax.all_to_all(summed, 'ep', split_axis=1, concat_axis=1, tiled=True)]
  transfers between devices with their start and end apart: 2 -> 0, of which waited for: 2 -> 0; matrix products, arithmetic and copies ran while one was open for 0% -> 0% of each run, Pallas kernels for 0% -> 0%
where the time goes in v1:
time: 25.7 us; the launch traced here: 25.5 us
  Pallas kernels  21.2 us (82%)
  local copies, waits for them, and re-layouts  4.26 us (17%)
    pallas_call x1, Pallas kernels, on_device(): pl.pallas_call(functools.partial(layer, ep, tp), out_shape=jax.ShapeDtype...  21.2 us
    unnamed x3, local copies, waits for them, and re-layouts  4.26 us

profile of v1, /device:TPU:0, one launch (start us, length us, event | category | flops | bytes accessed | tf_op | source)
XLA Modules:
  0.0 25.5 jit_solution(5574088088074836805)
XLA Ops:
  0.0 1.4 %copy.7.cho_hbm = s32[1,8,7]{2,1,0:T(8,128)} copy(s32[1,8,7]{1,0,2:T(1,128)} %param.7) | data formatting | bytes 448 | tf_op args[1]
  1.4 1.3 %copy.8.pw_hbm = f32[1,8,7]{2,1,0:T(8,128)} copy(f32[1,8,7]{1,0,2:T(1,128)} %param.8) | data formatting | bytes 448 | tf_op args[2]
  2.7 21.2 %shard_map.64 = bf16[128,512]{1,0:T(8,128)(2,1)} custom-call(bf16[128,2048]{1,0:T(8,128)(2,1)} %tok_hbm.1, s32[1,8,7]{2,1,0:T(8,128)} %copy.7.cho_hbm, f32[1,8,7]{2,1,0:T(8,128)} %copy.8.pw_hbm, bf16[1,2048,1024]{2,1,0:T(8,128)(2,1)} %gate_hbm.1, bf16[1,2048,1024]{2,1,0:T(8,128)(2,1)} %up_hbm.1, bf16[1,1024,2048]{2,1,0:T(8,128)(2,1)} %down_hbm.1), custom_call_target="tpu_custom_call" | custom-call | tf_op jit(solution)/shard_map/pallas_call | solution.py:198
  23.9 1.6 %copy.10 = bf16[128,512]{1,0:T(8,128)(2,1)} copy(bf16[128,512]{1,0:T(8,128)(2,1)} %shard_map.64) | data formatting | bytes 262144

commit v2 on v1

v2 whole, which is shorter than its diff:
```python
import functools
import jax
import jax.numpy as jnp
from jax import lax
from jax.experimental import pallas as pl
from jax.experimental.pallas import tpu as pltpu
from jax.sharding import PartitionSpec as P

F32 = jnp.float32
BF16 = jnp.bfloat16
PAD = 8


def each(n, f):
    if n <= 16:
        for i in range(n):
            f(i)
    else:
        lax.fori_loop(0, n, lambda i, s: (f(i), s)[1], 0)


def layer(
    ep, tp, tok_hbm, cho_hbm, pw_hbm, gate_hbm, up_hbm, down_hbm, out_ref,
    tok, cho, pw, gate, up, down, send1, x_own, x_sib, acc_g, acc_u, hid,
    send2, recv2, mine, send3, recv3, comb,
    in_sem, w_sem, s1_sem, r1_sem, s2_sem, r2_sem, s3_sem, r3_sem, s4_sem, r4_sem, ready,
):
    slots = cho.shape[0]
    toks, half = tok.shape
    parts, part_w = send1.shape[0], send1.shape[3]
    hidden = hid.shape[1]
    blk = out_ref.shape[1]
    ny = tp // 2
    e_me = lax.axis_index("ep")
    t_me = lax.axis_index("tp")
    y_me, c_me = t_me // 2, t_me % 2
    sib = y_me * 2 + (1 - c_me)
    own_k = pl.multiple_of(c_me * half, 128)
    sib_k = pl.multiple_of((1 - c_me) * half, 128)

    small = [
        pltpu.make_async_copy(cho_hbm, cho, in_sem.at[0]),
        pltpu.make_async_copy(pw_hbm, pw, in_sem.at[1]),
        pltpu.make_async_copy(tok_hbm.at[:, pl.ds(own_k, half)], tok, in_sem.at[2]),
    ]
    for c in small:
        c.start()

    barrier = pltpu.get_barrier_semaphore()
    near = ep // 2

    def peer(k):
        lower, pos = e_me // near, lax.rem(e_me, near)
        far = k < near
        base = jnp.where(far, 1 - lower, lower) * near
        return base + lax.rem(pos + jnp.where(far, k, k - near + 1), near)

    def hello(sem, **to):
        pl.semaphore_signal(sem, inc=1, device_id=to, device_id_type=pl.DeviceIdType.MESH)

    def beside(k):
        return lax.rem(y_me + 1 + k, ny) * 2 + c_me

    each(ep - 1, lambda k: hello(barrier, ep=peer(k)))
    each(ny - 1, lambda k: hello(barrier, tp=beside(k)))
    hello(barrier, tp=sib)

    weights = [
        pltpu.make_async_copy(gate_hbm.at[0, pl.ds(own_k, half)], gate.at[pl.ds(own_k, half)], w_sem.at[0]),
        pltpu.make_async_copy(up_hbm.at[0, pl.ds(own_k, half)], up.at[pl.ds(own_k, half)], w_sem.at[1]),
        pltpu.make_async_copy(gate_hbm.at[0, pl.ds(sib_k, half)], gate.at[pl.ds(sib_k, half)], w_sem.at[2]),
        pltpu.make_async_copy(up_hbm.at[0, pl.ds(sib_k, half)], up.at[pl.ds(sib_k, half)], w_sem.at[3]),
        pltpu.make_async_copy(down_hbm.at[0], down, w_sem.at[4]),
    ]
    for c in weights:
        c.start()

    small[0].wait()
    small[1].wait()
    here = lax.broadcasted_iota(jnp.int32, (PAD, toks), 1)
    lane = lax.broadcasted_iota(jnp.int32, (PAD, ep), 1)
    ids_all = jnp.concatenate(
        [cho[s] for s in range(slots)] + [jnp.full((1, ep), -1, jnp.int32)] * (PAD - slots), axis=0)
    val_all = jnp.concatenate(
        [pw[s] for s in range(slots)] + [jnp.zeros((1, ep), F32)] * (PAD - slots), axis=0)
    hot, wgt = [], []
    for e in range(ep):
        ids = jnp.sum(jnp.where(lane == e, ids_all, 0), axis=1, keepdims=True)
        val = jnp.sum(jnp.where(lane == e, val_all, 0.0), axis=1, keepdims=True)
        hit = here == ids
        hot.append(jnp.where(hit, 1.0, 0.0))
        wgt.append(jnp.where(hit, val, 0.0))
    hot = jnp.concatenate(hot, axis=0).astype(BF16)
    small[2].wait()
    for q in range(parts):
        picked = jnp.dot(hot, tok[:, q * part_w:(q + 1) * part_w], preferred_element_type=F32)
        send1[q] = picked.reshape(ep, PAD, part_w).astype(BF16)
        x_own[q, e_me] = send1[q, e_me]

    pl.semaphore_wait(barrier, ep + ny - 1)

    def copy1(q, to, slot):
        return pltpu.make_async_remote_copy(
            src_ref=send1.at[q, to], dst_ref=x_own.at[q, slot], send_sem=s1_sem, recv_sem=r1_sem.at[q, slot],
            device_id={"ep": to}, device_id_type=pl.DeviceIdType.MESH)

    for q in range(parts):
        each(ep - 1, lambda k, q=q: copy1(q, peer(k), e_me).start())
    each(ny - 1, lambda k: hello(ready, tp=beside(k)))

    wgt = jnp.concatenate(wgt, axis=0)
    hi = wgt.astype(BF16).astype(F32)
    mid = (wgt - hi).astype(BF16).astype(F32)
    lo = (wgt - hi) - mid
    comb[...] = jnp.transpose(jnp.concatenate([hi, mid, lo], axis=0)).astype(BF16)

    def pair_rows(q, src):
        return pltpu.make_async_remote_copy(
            src_ref=x_own.at[q, src], dst_ref=x_sib.at[q, src], send_sem=s2_sem, recv_sem=r2_sem.at[q],
            device_id={"tp": sib}, device_id_type=pl.DeviceIdType.MESH)

    def relay(q):
        def one(k):
            src = peer(k)
            copy1(q, src, src).wait_recv()
            pair_rows(q, src).start()

        pair_rows(q, e_me).start()
        each(near - 1, lambda k: one(k + near))
        each(near, one)

    def rows(ref, q):
        return ref[q].astype(F32).reshape(ep * PAD, part_w).astype(BF16)

    step = min(256, hidden)
    cols = [slice(j, j + step) for j in range(0, hidden, step)]

    def product(x, k0, first=False, final=False):
        at = pl.ds(pl.multiple_of(k0, 128), part_w)
        for c in cols:
            g = jnp.dot(x, gate[at, c], preferred_element_type=F32)
            u = jnp.dot(x, up[at, c], preferred_element_type=F32)
            if not first:
                g, u = g + acc_g[:, c], u + acc_u[:, c]
            if final:
                hid[:, c] = (g / (1.0 + jnp.exp(-g)) * u).astype(BF16)
            else:
                acc_g[:, c], acc_u[:, c] = g, u

    relay(0)
    weights[0].wait()
    weights[1].wait()
    product(rows(x_own, 0), own_k, first=True)
    for q in range(parts):
        if q + 1 < parts:
            relay(q + 1)
        if q == 0:
            weights[2].wait()
            weights[3].wait()
        else:
            product(rows(x_own, q), own_k + q * part_w)
        pltpu.make_async_remote_copy(
            src_ref=x_own.at[q], dst_ref=x_sib.at[q], send_sem=s2_sem, recv_sem=r2_sem.at[q],
            device_id={"tp": sib}, device_id_type=pl.DeviceIdType.MESH).wait_recv()
        product(rows(x_sib, q), sib_k + q * part_w, final=q == parts - 1)
    h = hid[...]
    weights[4].wait()
    if ny > 1:
        pl.semaphore_wait(ready, ny - 1)

    def part(f):
        return jnp.dot(h, down[:, pl.ds(pl.multiple_of(f * blk, 128), blk)], preferred_element_type=F32)

    def pair_copy(i):
        return pltpu.make_async_remote_copy(
            src_ref=send2.at[i], dst_ref=recv2.at[i], send_sem=s3_sem.at[i], recv_sem=r3_sem.at[i],
            device_id={"tp": sib}, device_id_type=pl.DeviceIdType.MESH)

    for i in range(ny):
        y = lax.rem(y_me + 1 + i, ny)
        send2[i] = part(y * 2 + (1 - c_me)).astype(BF16)
        pair_copy(i).start()
    for i in range(ny):
        y = lax.rem(y_me + 1 + i, ny)
        mine[...] = part(y * 2 + c_me)
        pair_copy(i).wait_recv()
        total = mine[...] + recv2[i].astype(F32)
        send3[i] = total.reshape(ep, PAD, blk).astype(BF16)

        def give(k, i=i, y=y):
            to = peer(k)
            pltpu.make_async_remote_copy(
                src_ref=send3.at[i, to], dst_ref=recv3.at[y_me, e_me], send_sem=s4_sem, recv_sem=r4_sem,
                device_id={"ep": to, "tp": y * 2 + c_me}, device_id_type=pl.DeviceIdType.MESH).start()

        each(ep - 1 if i == ny - 1 else ep, give)
    pltpu.make_async_copy(send3.at[ny - 1, e_me], recv3.at[y_me, e_me], r4_sem).start()

    sent = send1.at[:, pl.ds(0, ep - 1)]
    pltpu.make_async_copy(sent, sent, s1_sem).wait()
    pltpu.make_async_copy(x_own, x_own, s2_sem).wait()
    for i in range(ny):
        pair_copy(i).wait_send()
    pltpu.make_async_copy(recv3, recv3, r4_sem).wait()
    total = recv3[0].astype(F32)
    for y in range(1, ny):
        total = total + recv3[y].astype(F32)
    r = total.reshape(ep * PAD, blk).astype(BF16)
    out_ref[...] = jnp.dot(
        comb[...], jnp.concatenate([r, r, r], axis=0), preferred_element_type=F32).astype(BF16)
    if ny > 1:
        pltpu.make_async_copy(send3.at[pl.ds(0, ny - 1)], send3.at[pl.ds(0, ny - 1)], s4_sem).wait()
    pltpu.make_async_copy(send3.at[0, pl.ds(0, ep - 1)], send3.at[0, pl.ds(0, ep - 1)], s4_sem).wait()


def on_device(ep, tp, tokens, chosen, pick_weight, gate_weight, up_weight, down_weight):
    toks, width = tokens.shape
    chosen = jnp.transpose(chosen, (2, 0, 1))
    pick_weight = jnp.transpose(pick_weight, (2, 0, 1))
    hidden = gate_weight.shape[2]
    half, blk, ny, rows = width // 2, width // tp, tp // 2, ep * PAD
    parts = 2
    dma = pltpu.SemaphoreType.DMA
    return pl.pallas_call(
        functools.partial(layer, ep, tp),
        out_shape=pltpu.VMEM((toks, blk), tokens.dtype),
        in_specs=[pl.BlockSpec(memory_space=pl.ANY)] * 6,
        out_specs=pl.BlockSpec(memory_space=pltpu.VMEM),
        scratch_shapes=[
            pltpu.VMEM((toks, half), BF16),
            pltpu.VMEM(chosen.shape, jnp.int32),
            pltpu.VMEM(pick_weight.shape, F32),
            pltpu.VMEM((width, hidden), BF16),
            pltpu.VMEM((width, hidden), BF16),
            pltpu.VMEM((hidden, width), BF16),
            pltpu.VMEM((parts, ep, PAD, half // parts), BF16),
            pltpu.VMEM((parts, ep, PAD, half // parts), BF16),
            pltpu.VMEM((parts, ep, PAD, half // parts), BF16),
            pltpu.VMEM((rows, hidden), F32),
            pltpu.VMEM((rows, hidden), F32),
            pltpu.VMEM((rows, hidden), BF16),
            pltpu.VMEM((ny, rows, blk), BF16),
            pltpu.VMEM((ny, rows, blk), BF16),
            pltpu.VMEM((rows, blk), F32),
            pltpu.VMEM((ny, ep, PAD, blk), BF16),
            pltpu.VMEM((ny, ep, PAD, blk), BF16),
            pltpu.VMEM((toks, 3 * rows), BF16),
            dma((3,)), dma((5,)), dma, dma((parts, ep)), dma, dma((parts,)), dma((ny,)), dma((ny,)), dma, dma,
            pltpu.SemaphoreType.REGULAR,
        ],
        compiler_params=pltpu.CompilerParams(
            collective_id=0, has_side_effects=True, vmem_limit_bytes=60 * 1024 * 1024),
    )(tokens, chosen, pick_weight, gate_weight, up_weight, down_weight)


def solution(mesh):
    ep, tp = mesh.shape["ep"], mesh.shape["tp"]
    return jax.shard_map(
        functools.partial(on_device, ep, tp),
        mesh=mesh,
        in_specs=(
            P("ep", None),
            P("ep", None, None),
            P("ep", None, None),
            P("ep", None, "tp"),
            P("ep", None, "tp"),
            P("ep", "tp", None),
        ),
        out_specs=P("ep", "tp"),
        check_vma=False,
    )
```

time: 25.7 us -> 20.3 us (0.79)
  local copies, waits for them, and re-layouts: 4.26 us -> 0.66 us
  Pallas kernels: 21.2 us -> 19.5 us
    unnamed x3 -> x1, local copies, waits for them, and re-layouts: 4.26 us -> 0.66 us
    pallas_call x1, Pallas kernels: 21.2 us -> 19.5 us  [on_device(): pl.pallas_call(functools.partial(layer, ep, tp), out_shape=pltpu.VMEM((to...]
where the time goes in v2:
time: 20.3 us; the launch traced here: 20.1 us
  Pallas kernels  19.5 us (96%)
  local copies, waits for them, and re-layouts  0.66 us (3%)
    pallas_call x1, Pallas kernels, on_device(): pl.pallas_call(functools.partial(layer, ep, tp), out_shape=pltpu.VMEM((to...  19.5 us
    unnamed x1, local copies, waits for them, and re-layouts  0.66 us

profile of v2, /device:TPU:0, one launch (start us, length us, event | category | flops | bytes accessed | tf_op | source)
XLA Modules:
  0.0 20.1 jit_solution(13290768241730956781)
XLA Ops:
  0.0 19.5 %shard_map.64 = bf16[128,512]{1,0:T(8,128)(2,1)S(1)} custom-call(bf16[128,2048]{1,0:T(8,128)(2,1)} %tok_hbm.1, s32[7,1,8]{2,1,0:T(1,128)} %bitcast.2, f32[7,1,8]{2,1,0:T(1,128)} %bitcast.3, bf16[1,2048,1024]{2,1,0:T(8,128)(2,1)} %gate_hbm.1, bf16[1,2048,1024]{2,1,0:T(8,128)(2,1)} %up_hbm.1, bf16[1,1024,2048]{2,1,0:T(8,128)(2,1)} %down_hbm.1), custom_call_target="tpu_custom_call" | custom-call | tf_op jit(solution)/shard_map/pallas_call | solution.py:224
  19.5 0.7 %copy.8 = bf16[128,512]{1,0:T(8,128)(2,1)} copy(bf16[128,512]{1,0:T(8,128)(2,1)S(1)} %shard_map.64) | data formatting | bytes 262144

commit v3 on v2

--- a/solution.py
+++ b/solution.py
@@ -49,17 +49,24 @@
     barrier = pltpu.get_barrier_semaphore()
     near = ep // 2
 
+    lower = (e_me >= near).astype(jnp.int32)
+    mine0, other0 = lower * near, (1 - lower) * near
+    pos = e_me - mine0
+
+    def wrap(v, n):
+        return jnp.where(v >= n, v - n, v)
+
     def peer(k):
-        lower, pos = e_me // near, lax.rem(e_me, near)
+        if isinstance(k, int):
+            return other0 + wrap(pos + k, near) if k < near else mine0 + wrap(pos + k - near + 1, near)
         far = k < near
-        base = jnp.where(far, 1 - lower, lower) * near
-        return base + lax.rem(pos + jnp.where(far, k, k - near + 1), near)
+        return jnp.where(far, other0, mine0) + wrap(pos + jnp.where(far, k, k - near + 1), near)
 
     def hello(sem, **to):
         pl.semaphore_signal(sem, inc=1, device_id=to, device_id_type=pl.DeviceIdType.MESH)
 
     def beside(k):
-        return lax.rem(y_me + 1 + k, ny) * 2 + c_me
+        return wrap(y_me + 1 + k, ny) * 2 + c_me
 
     each(ep - 1, lambda k: hello(barrier, ep=peer(k)))
     each(ny - 1, lambda k: hello(barrier, tp=beside(k)))
@@ -177,11 +184,11 @@
             device_id={"tp": sib}, device_id_type=pl.DeviceIdType.MESH)
 
     for i in range(ny):
-        y = lax.rem(y_me + 1 + i, ny)
+        y = wrap(y_me + 1 + i, ny)
         send2[i] = part(y * 2 + (1 - c_me)).astype(BF16)
         pair_copy(i).start()
     for i in range(ny):
-        y = lax.rem(y_me + 1 + i, ny)
+        y = wrap(y_me + 1 + i, ny)
         mine[...] = part(y * 2 + c_me)
         pair_copy(i).wait_recv()
         total = mine[...] + recv2[i].astype(F32)

time: 20.3 us -> 20.3 us (level)
  no operation moved by 1% of the time
where the time goes in v3:
time: 20.3 us; the launch traced here: 20.1 us
  Pallas kernels  19.5 us (96%)
  local copies, waits for them, and re-layouts  0.66 us (3%)
    pallas_call x1, Pallas kernels, on_device(): pl.pallas_call(functools.partial(layer, ep, tp), out_shape=pltpu.VMEM((to...  19.5 us
    unnamed x1, local copies, waits for them, and re-layouts  0.66 us

profile of v3, /device:TPU:0, one launch (start us, length us, event | category | flops | bytes accessed | tf_op | source)
XLA Modules:
  0.0 20.1 jit_solution(5338245518880990099)
XLA Ops:
  0.0 19.5 %shard_map.64 = bf16[128,512]{1,0:T(8,128)(2,1)S(1)} custom-call(bf16[128,2048]{1,0:T(8,128)(2,1)} %tok_hbm.1, s32[7,1,8]{2,1,0:T(1,128)} %bitcast.2, f32[7,1,8]{2,1,0:T(1,128)} %bitcast.3, bf16[1,2048,1024]{2,1,0:T(8,128)(2,1)} %gate_hbm.1, bf16[1,2048,1024]{2,1,0:T(8,128)(2,1)} %up_hbm.1, bf16[1,1024,2048]{2,1,0:T(8,128)(2,1)} %down_hbm.1), custom_call_target="tpu_custom_call" | custom-call | tf_op jit(solution)/shard_map/pallas_call | solution.py:231
  19.5 0.7 %copy.8 = bf16[128,512]{1,0:T(8,128)(2,1)} copy(bf16[128,512]{1,0:T(8,128)(2,1)S(1)} %shard_map.64) | data formatting | bytes 262144
